TPU v7x, 512 devices: a whole 4x8x8 slice. The times are simulated.
512 devices in a mesh: sp: 32 (over z, x), tp: 16 (over y, core).
Axes of the slice: x: 4, y: 8, z: 8, core: 2. Of those that a mesh axis runs over, the one named last changes fastest.
Arguments:
- residual_in: bfloat16 [6144, 2048], P('sp', 'tp'), may hold values from -6 to 6
- query_rows: bfloat16 [6144, 1024], P('sp', 'tp'), may hold values from -8 to 8
- key_rows: bfloat16 [6144, 1024], P('sp', 'tp'), may hold values from -8 to 8
- value_rows: bfloat16 [6144, 1024], P('sp', 'tp'), may hold values from -6 to 6
- map_weight: float32 [16], P('tp'), may hold values from 0.3 to 0.8
- head_gain: float32 [64], replicated, may hold values from 0.1 to 1.9
- out_proj: bfloat16 [1024, 2048], P(None, 'tp'), may hold values from -0.1875 to 0.1875
- norm_gain: float32 [2048], replicated, may hold values from 0.1 to 1.9
- route_ids: int32 [6144, 2], P('sp'), may hold values from 0 to 31, all different within a row; in each aligned block of 192 rows (0 to 191, 192 to 383, ...) at most 15 rows name the same one
- route_weights: float32 [6144, 2], P('sp'), may hold values from 0.2 to 1.2
- expert_gate: bfloat16 [32, 1024, 2048], P('sp', 'tp'), may hold values from -0.125 to 0.125
- expert_up: bfloat16 [32, 1024, 2048], P('sp', 'tp'), may hold values from -0.125 to 0.125
- expert_down: bfloat16 [32, 1024, 2048], P('sp', None, 'tp'), may hold values from -0.1875 to 0.1875
- shared_gate: bfloat16 [1024, 2048], P('tp'), may hold values from -0.125 to 0.125
- shared_up: bfloat16 [1024, 2048], P('tp'), may hold values from -0.125 to 0.125
- shared_down: bfloat16 [1024, 2048], P(None, 'tp'), may hold values from -0.1875 to 0.1875
Outputs:
- mixed_out: bfloat16 [6144, 2048], P('sp', 'tp')
Inputs may be any that keep to these rules, and one draw needn't show every extreme that they name: `route_ids`: each row names 2 different experts. Among the rows held by one index of sp no expert is named more than 15 times, and in every draw some expert is named exactly 15 times by the rows of some index of sp.
All inputs are finite; a program needn't handle non-finite values.
Results may differ from a plain program's by a relative error of at most 0.0095.
Values may be sent and summed in bfloat16 or wider, within the bound.
A program may use at most 64 MiB of HBM per device.

v0:
```python
import jax
import jax.numpy as jnp
from jax import lax
from jax.sharding import PartitionSpec as P

epsilon = 1e-06
masked_score = -1e30


def in_order(tiles, dim):
    tiles = jnp.moveaxis(tiles, 0, dim)
    lengths = tiles.shape
    return tiles.reshape(*lengths[:dim], lengths[dim] * lengths[dim + 1], *lengths[dim + 2 :])


def copy_for_each(value, axis):
    copies = jnp.broadcast_to(value, (lax.axis_size(axis), *value.shape))
    return lax.all_to_all(copies, axis, split_axis=0, concat_axis=0, tiled=True)


def gathered_copies(value, axis, dim):
    return in_order(copy_for_each(value, axis), dim)


def in_one_piece(arrays, axis, dim, along):
    ends, at = ([], 0)
    for a in arrays[:-1]:
        at += a.shape[along]
        ends.append(at)
    both = jnp.concatenate(arrays, axis=along)
    return tuple(jnp.split(gathered_copies(both, axis, dim), ends, axis=along))


def turned_gather(arrays, axis, dims):
    turned = [jnp.moveaxis(a, dim, 0) for a, dim in zip(arrays, dims)]
    widths = [t[0].size for t in turned]
    both = jnp.concatenate([t.reshape(-1, w) for t, w in zip(turned, widths)], axis=1)
    out = lax.all_gather(both, axis, axis=0, tiled=True)
    tiles = jnp.split(out, [sum(widths[:k]) for k in range(1, len(widths))], axis=1)
    return tuple(
        (
            jnp.moveaxis(b.reshape(-1, *t.shape[1:]), 0, dim)
            for b, t, dim in zip(tiles, turned, dims)
        )
    )


def rms_scale(values, gain_vec):
    squares = jnp.mean(values * values, axis=-1, keepdims=True)
    return values * lax.rsqrt(squares + epsilon) * gain_vec


def block_slots(route_block, experts_all, capacity):
    flat_ids = route_block.reshape(-1)
    one_hot = (flat_ids[:, None] == jnp.arange(experts_all, dtype=jnp.int32)[None, :]).astype(
        jnp.int32
    )
    earlier = jnp.cumsum(one_hot, axis=0) - one_hot
    position = jnp.sum(earlier * one_hot, axis=1)
    return (flat_ids * capacity + position).reshape(route_block.shape)


def body(
    residual_in,
    query_rows,
    key_rows,
    value_rows,
    map_weight,
    head_gain,
    out_proj,
    norm_gain,
    route_ids,
    route_weights,
    expert_gate,
    expert_up,
    expert_down,
    shared_gate,
    shared_up,
    shared_down,
):
    seq_dev = residual_in.shape[0]
    col_dev = residual_in.shape[1]
    heads_here = map_weight.shape[0]
    head_dim = head_gain.shape[0]
    half_dim = head_dim // 2
    topk_count = route_ids.shape[1]
    exp_here = expert_gate.shape[0]
    experts_all = exp_here * lax.axis_size("sp")
    capacity = 5 * seq_dev * topk_count // (4 * experts_all)
    score_scale = half_dim ** (-0.5)
    query_pos = lax.axis_index("sp") * seq_dev + jnp.arange(seq_dev, dtype=jnp.int32)
    query_heads = query_rows.reshape(seq_dev, heads_here, 2, half_dim)
    key_piece, value_piece = in_one_piece((key_rows, value_rows), "sp", 0, 1)
    piece_len = key_piece.shape[0]
    key_heads = key_piece.reshape(piece_len, heads_here, 2, half_dim)
    value_heads = value_piece.reshape(piece_len, heads_here, head_dim)
    scores = (
        jnp.einsum("qhmd,khmd->mhqk", query_heads, key_heads, preferred_element_type=jnp.float32)
        * score_scale
    )
    key_pos = jnp.arange(piece_len, dtype=jnp.int32)
    visible = key_pos[None, :] <= query_pos[:, None]
    scores = jnp.where(visible, scores, masked_score)
    run_max = jnp.full((2, heads_here, seq_dev), masked_score, jnp.float32)
    new_max = jnp.maximum(run_max, jnp.max(scores, axis=-1))
    expo = jnp.where(visible, jnp.exp(scores - new_max[..., None]), 0.0)
    new_sum = jnp.sum(expo, axis=-1)
    product = jnp.einsum(
        "mhqk,khd->mhqd", expo.astype(jnp.bfloat16), value_heads, preferred_element_type=jnp.float32
    )
    summed = product / new_sum[..., None]
    diff_out = summed[0] - map_weight[:, None, None] * summed[1]
    head_out = rms_scale(diff_out, head_gain).astype(jnp.bfloat16)
    head_out = jnp.transpose(head_out, (1, 0, 2)).reshape(seq_dev, heads_here * head_dim)
    attn = jnp.dot(
        lax.all_gather(head_out, "tp", axis=1, tiled=True),
        out_proj,
        preferred_element_type=jnp.float32,
    )
    hidden_state = (residual_in.astype(jnp.float32) + attn).astype(jnp.bfloat16)
    full_rows = lax.all_gather(hidden_state, "tp", axis=1, tiled=True)
    normed = rms_scale(full_rows.astype(jnp.float32), norm_gain).astype(jnp.bfloat16)
    shared_gate_part = jnp.einsum(
        "rd,fd->rf", normed, shared_gate, preferred_element_type=jnp.float32
    )
    shared_up_part = jnp.einsum("rd,fd->rf", normed, shared_up, preferred_element_type=jnp.float32)
    shared_hidden = (jax.nn.silu(shared_gate_part) * shared_up_part).astype(jnp.bfloat16)
    slot_ids = block_slots(route_ids, experts_all, capacity)
    token_of = jnp.repeat(jnp.arange(seq_dev, dtype=jnp.int32), topk_count)
    slot_token = (
        jnp.full((experts_all * capacity,), seq_dev, jnp.int32)
        .at[slot_ids.reshape(-1)]
        .set(token_of)
    )
    own_cols = lax.dynamic_slice_in_dim(normed, lax.axis_index("tp") * col_dev, col_dev, 1)
    padded = jnp.concatenate([own_cols, jnp.zeros((1, col_dev), jnp.bfloat16)], axis=0)
    outgoing = jnp.take(padded, slot_token, axis=0).reshape(experts_all, capacity, col_dev)
    arrived = lax.all_to_all(outgoing, "sp", split_axis=0, concat_axis=1, tiled=True)
    arrived_rows = arrived.shape[1]
    pieces = lax.all_gather(arrived, "tp", axis=2, tiled=True)
    gate_add = jnp.einsum("erd,efd->erf", pieces, expert_gate, preferred_element_type=jnp.float32)
    up_add = jnp.einsum("erd,efd->erf", pieces, expert_up, preferred_element_type=jnp.float32)
    expert_hidden = (jax.nn.silu(gate_add) * up_add).astype(jnp.bfloat16)
    expert_flat = expert_hidden.reshape(exp_here * arrived_rows, expert_hidden.shape[2])
    pieces = turned_gather((shared_hidden, expert_flat), "tp", (1, 1))
    piece_width = pieces[0].shape[1]
    routed_piece = pieces[1].reshape(exp_here, arrived_rows, piece_width)
    shared_add = jnp.dot(pieces[0], shared_down, preferred_element_type=jnp.float32)
    expert_add = jnp.einsum(
        "erf,efd->erd", routed_piece, expert_down, preferred_element_type=jnp.float32
    )
    returned_rows = lax.all_to_all(
        expert_add.astype(jnp.bfloat16), "sp", split_axis=1, concat_axis=0, tiled=True
    )
    returned_flat = returned_rows.reshape(experts_all * capacity, col_dev)
    picked = (
        jnp.take(returned_flat, slot_ids.reshape(-1), axis=0)
        .reshape(seq_dev, topk_count, col_dev)
        .astype(jnp.float32)
    )
    routed = jnp.sum(picked * route_weights[:, :, None], axis=1)
    return (hidden_state.astype(jnp.float32) + shared_add + routed).astype(jnp.bfloat16)


def solution(mesh):
    in_specs = (
        P("sp", "tp"),
        P("sp", "tp"),
        P("sp", "tp"),
        P("sp", "tp"),
        P("tp"),
        P(),
        P(None, "tp"),
        P(),
        P("sp", None),
        P("sp", None),
        P("sp", "tp", None),
        P("sp", "tp", None),
        P("sp", None, "tp"),
        P("tp", None),
        P("tp", None),
        P(None, "tp"),
    )
    out_specs = P("sp", "tp")
    return jax.shard_map(body, mesh=mesh, in_specs=in_specs, out_specs=out_specs, check_vma=False)
```

profile of v0, /device:TPU:1, one launch (start us, length us, event | category | flops | bytes accessed | tf_op | source)
XLA Modules:
  0.0 245.5 jit_solution(9323210374195220313)
XLA Ops:
  6.5 0.8 pad_maximum_fusion.1
  7.5 1.5 broadcast_in_dim.61
  9.0 13.8 %all-to-all-start = ((bf16[32,192,128]{2,1,0:T(8,128)(2,1)}), bf16[32,192,128]{2,1,0:T(8,128)(2,1)S(1)}, u32[]{:S(2)}, u32[]{:S(2)}) async-start(bf16[32,192,128]{2,1,0:T(8,128)(2,1)} %broadcast_in_dim.61), calls=%async_computation | async-start | bytes 3145728 | tf_op jit(solution)/shard_map/all_to_all | solution.py:18
  24.0 0.9 reduce-window.6
  25.7 2.9 %scatter_custom_fusion = s32[480]{0:T(512)S(1)} fusion(s32[384]{0:T(512)S(1)} %fusion.53, s32[384]{0:T(512)S(1)} %reshape.274, s32[]{:T(128)} %constant.26.clone.1), kind=kCustom, calls=%fused_computation.75 | custom fusion | bytes 1924 | tf_op jit(solution)/shard_map/scatter | solution.py:133
  28.8 0.8 iota_compare_fusion
  29.6 31.1 %all-to-all-done = bf16[32,192,128]{2,1,0:T(8,128)(2,1)S(1)} async-done(((bf16[32,192,128]{2,1,0:T(8,128)(2,1)}), bf16[32,192,128]{2,1,0:T(8,128)(2,1)S(1)}, u32[]{:S(2)}, u32[]{:S(2)}) %all-to-all-start) | async-done | bytes 1572896 | tf_op jit(solution)/shard_map/all_to_all | solution.py:18
  60.7 1.4 copy.47
  62.2 3.5 %fusion.57 = (f32[2,192]{1,0:T(2,128)S(1)}, f32[2,192,6144]{2,1,0:T(8,128)S(1)}) fusion(bf16[6144,2,32]{0,2,1:T(8,128)(2,1)} %bitcast.115, bf16[192,2,32]{0,2,1:T(8,128)(2,1)S(1)} %bitcast.118, pred[192,6144]{1,0:T(8,128)(4,1)S(1)} %iota_compare_fusion), kind=kOutput, calls=%fused_computation.83 | convolution fusion | flops 158072448 | bytes 11429376 | tf_op jit(solution)/shard_map/qhmd,khmd->mhqk/dot_general | solution.py:98
  65.7 2.5 %fusion = f32[2,192]{1,0:T(2,128)S(1)} fusion(f32[2,192,6144]{2,1,0:T(8,128)S(1)} %get-tuple-element.6, f32[2,192]{1,0:T(2,128)S(1)} %broadcast_maximum_fusion, pred[192,6144]{1,0:T(8,128)(4,1)S(1)} %iota_compare_fusion), kind=kLoop, calls=%fused_computation.5 | loop fusion | flops 7077504 | bytes 10619904 | tf_op jit(solution)/shard_map/reduce_sum | solution.py:107
  68.3 2.7 %fusion.38 = f32[2,1,192,64]{2,3,0,1:T(8,128)S(1)} fusion(f32[2,192,6144]{2,1,0:T(8,128)S(1)} %get-tuple-element.6, f32[2,192]{1,0:T(2,128)S(1)} %broadcast_maximum_fusion, pred[192,6144]{1,0:T(8,128)(4,1)S(1)} %iota_compare_fusion, bf16[6144,128]{1,0:T(8,128)(2,1)S(1)} %bitcast.112, f32[2,192]{1,0:T(2,128)S(1)} %fusion), kind=kOutput, calls=%fused_computation.39 | convolution fusion | flops 309092352 | bytes 12291072 | tf_op jit(solution)/shard_map/mhqk,khd->mhqd/dot_general | solution.py:108
  71.1 21.0 %all_gather.12 = bf16[192,1024]{0,1:T(8,128)(2,1)S(1)} all-gather(bf16[192,64]{0,1:T(8,128)(2,1)S(1)} %fusion.48), channel_id=1, replica_groups=mesh['sp'=32,'tp'=16] {'tp'}, dimensions={1}, use_global_device_ids=true | all-gather | bytes 417792 | tf_op jit(solution)/shard_map/all_gather | solution.py:116
  92.4 17.1 %all_gather.13 = bf16[192,2048]{1,0:T(8,128)(2,1)S(1)} all-gather(bf16[192,128]{1,0:T(8,128)(2,1)S(1)} %fusion.31), channel_id=1, replica_groups=mesh['sp'=32,'tp'=16] {'tp'}, dimensions={1}, use_global_device_ids=true | all-gather | bytes 835584 | tf_op jit(solution)/shard_map/all_gather | solution.py:121
  110.1 1.5 gather_fusion
  111.8 15.2 %all_to_all.26 = bf16[32,15,128]{2,1,0:T(8,128)(2,1)S(1)} all-to-all(bf16[32,15,128]{2,1,0:T(8,128)(2,1)S(1)} %broadcast_select_fusion.1), channel_id=1, replica_groups=mesh['sp'=32,'tp'=16] {'sp'}, dimensions={0} | all-to-all | bytes 245760 | tf_op jit(solution)/shard_map/all_to_all | solution.py:138
  127.0 0.7 all_to_all.10
  127.8 0.4 convolution_bitcast_fusion.1
  128.2 0.4 fusion.34
  128.6 36.1 %all-gather.3.cloned.1.call-done = bf16[1,480,2048]{2,1,0:T(8,128)(2,1)} async-done(((bf16[1,480,128]{2,1,0:T(8,128)(2,1)}), bf16[1,480,2048]{2,1,0:T(8,128)(2,1)}) %all-gather.3.cloned.1.call-update) | async-done | bytes 1966096 | tf_op jit(solution)/shard_map/all_gather | solution.py:140
  164.8 2.4 fusion.17
  167.2 0.7 fusion.27
  167.9 0.7 pad_maximum_fusion
  168.9 40.5 %all-gather.5.cloned.1.call-done = bf16[1024,672]{1,0:T(8,128)(2,1)} async-done(((bf16[64,672]{1,0:T(8,128)(2,1)}), bf16[1024,672]{1,0:T(8,128)(2,1)}) %all-gather.5.cloned.1.call-update) | async-done | bytes 1376272 | tf_op jit(solution)/shard_map/all_gather | solution.py:38
  209.4 2.2 fusion.26
  211.8 0.5 broadcast.160
  212.3 1.4 reduce.10
  213.7 0.8 reshape.284
  214.5 9.9 %all-to-all-start.2 = ((bf16[32,2,960]{2,1,0:T(2,128)(2,1)}), bf16[32,2,960]{2,1,0:T(2,128)(2,1)S(1)}, u32[]{:S(2)}, u32[]{:S(2)}) async-start(bf16[32,2,960]{2,1,0:T(2,128)(2,1)} %reshape.284), calls=%async_computation.2 | async-start | bytes 262144 | tf_op jit(solution)/shard_map/all_to_all | solution.py:152
  224.7 9.1 %all-to-all-done.2 = bf16[32,2,960]{2,1,0:T(2,128)(2,1)S(1)} async-done(((bf16[32,2,960]{2,1,0:T(2,128)(2,1)}), bf16[32,2,960]{2,1,0:T(2,128)(2,1)S(1)}, u32[]{:S(2)}, u32[]{:S(2)}) %all-to-all-start.2) | async-done | bytes 122912 | tf_op jit(solution)/shard_map/all_to_all | solution.py:152
  234.0 1.4 gather_fusion.1
  235.5 1.1 multiply_reduce_fusion
  236.6 2.0 fusion.32
  (72 shorter events, 3.7 us)
Async XLA Ops:
  6.5 202.9 %copy-start = (bf16[1,1024,128]{2,1,0:T(8,128)(2,1)S(1)}, bf16[1,1024,128]{2,1,0:T(8,128)(2,1)}, u32[]{:S(2)}) copy-start(bf16[1,1024,128]{2,1,0:T(8,128)(2,1)} %param.28) | copy-start | bytes 786436
  9.0 13.9 %copy-start.6 = (s32[192,2]{0,1:T(2,128)S(1)}, s32[192,2]{0,1:T(2,128)}, u32[]{:S(2)}) copy-start(s32[192,2]{0,1:T(2,128)} %param.24) | copy-start | bytes 4612
  9.0 51.7 %all-to-all-start = ((bf16[32,192,128]{2,1,0:T(8,128)(2,1)}), bf16[32,192,128]{2,1,0:T(8,128)(2,1)S(1)}, u32[]{:S(2)}, u32[]{:S(2)}) async-start(bf16[32,192,128]{2,1,0:T(8,128)(2,1)} %broadcast_in_dim.61), calls=%async_computation | async-start | bytes 3145728 | tf_op jit(solution)/shard_map/all_to_all | solution.py:18
  22.8 141.9 %all-gather.3.cloned.1.call-start = ((), (), s32[]{:S(2)}) async-start(), calls=%async_computation.3 | async-start | bytes 2088960 | tf_op jit(solution)/shard_map/all_gather | solution.py:140
  25.3 36.9 %copy-start.13 = (bf16[192,64]{0,1:T(8,128)(2,1)S(1)}, bf16[192,64]{0,1:T(8,128)(2,1)}, u32[]{:S(2)}) copy-start(bf16[192,64]{0,1:T(8,128)(2,1)} %param.17) | copy-start | bytes 73732
  68.2 2.7 %copy-start.9 = (f32[64]{0:T(128)S(1)}, f32[64]{0:T(128)}, u32[]{:S(2)}) copy-start(f32[64]{0:T(128)} %param.21) | copy-start | bytes 772
  68.2 23.9 %copy-start.2 = (bf16[1024,128]{1,0:T(8,128)(2,1)S(1)}, bf16[1024,128]{1,0:T(8,128)(2,1)}, u32[]{:S(2)}) copy-start(bf16[1024,128]{1,0:T(8,128)(2,1)} %param.22) | copy-start | bytes 786436
  68.3 23.9 %copy-start.5 = (bf16[192,128]{1,0:T(8,128)(2,1)S(1)}, bf16[192,128]{1,0:T(8,128)(2,1)}, u32[]{:S(2)}) copy-start(bf16[192,128]{1,0:T(8,128)(2,1)} %param.16) | copy-start | bytes 147460
  70.9 38.9 %copy-start.7 = (f32[2048]{0:T(1024)S(1)}, f32[2048]{0:T(1024)}, u32[]{:S(2)}) copy-start(f32[2048]{0:T(1024)} %param.23) | copy-start | bytes 24580
  109.8 18.1 %copy-start.3 = (bf16[64,2048]{1,0:T(8,128)(2,1)S(1)}, bf16[64,2048]{1,0:T(8,128)(2,1)}, u32[]{:S(2)}) copy-start(bf16[64,2048]{1,0:T(8,128)(2,1)} %param.29) | copy-start | bytes 786436
  110.0 18.2 %copy-start.10 = (bf16[64,2048]{1,0:T(8,128)(2,1)S(1)}, bf16[64,2048]{1,0:T(8,128)(2,1)}, u32[]{:S(2)}) copy-start(bf16[64,2048]{1,0:T(8,128)(2,1)} %param.30) | copy-start | bytes 786436
  111.6 53.1 %copy-start.4 = (bf16[1,64,2048]{2,1,0:T(8,128)(2,1)S(1)}, bf16[1,64,2048]{2,1,0:T(8,128)(2,1)}, u32[]{:S(2)}) copy-start(bf16[1,64,2048]{2,1,0:T(8,128)(2,1)} %param.26) | copy-start | bytes 786436
  127.8 81.7 %all-gather.5.cloned.1.call-start = ((), (), s32[]{:S(2)}) async-start(), calls=%async_computation.4 | async-start | bytes 1671168 | tf_op jit(solution)/shard_map/all_gather | solution.py:38
  128.2 38.9 %copy-start.11 = (bf16[1,64,2048]{2,1,0:T(8,128)(2,1)S(1)}, bf16[1,64,2048]{2,1,0:T(8,128)(2,1)}, u32[]{:S(2)}) copy-start(bf16[1,64,2048]{2,1,0:T(8,128)(2,1)} %param.27) | copy-start | bytes 786436
  164.8 2.4 copy-start.1
  167.9 56.6 %copy-start.8 = (f32[192,2]{0,1:T(2,128)S(1)}, f32[192,2]{0,1:T(2,128)}, u32[]{:S(2)}) copy-start(f32[192,2]{0,1:T(2,128)} %param.25) | copy-start | bytes 4612
  211.6 25.0 %copy-start.12 = (bf16[1024,128]{1,0:T(8,128)(2,1)S(1)}, bf16[1024,128]{1,0:T(8,128)(2,1)}, u32[]{:S(2)}) copy-start(bf16[1024,128]{1,0:T(8,128)(2,1)} %param.31) | copy-start | bytes 786436
  214.5 19.4 %all-to-all-start.2 = ((bf16[32,2,960]{2,1,0:T(2,128)(2,1)}), bf16[32,2,960]{2,1,0:T(2,128)(2,1)S(1)}, u32[]{:S(2)}, u32[]{:S(2)}) async-start(bf16[32,2,960]{2,1,0:T(2,128)(2,1)} %reshape.284), calls=%async_computation.2 | async-start | bytes 262144 | tf_op jit(solution)/shard_map/all_to_all | solution.py:152
Sparse Core Ops, SparseCore 0:
  127.9 36.8 all-gather.2
  168.8 40.5 all-gather.4
where the time goes:
time: 246 us; the launch traced here: 245 us
  waiting for transfers between devices  117 us (48%)
  blocking collectives  53.3 us (22%)
  starting transfers between devices  23.8 us (10%)
  matrix products  14.5 us (6%)
  between operations  14.5 us (6%)
  local copies, waits for them, and re-layouts  13.1 us (5%)
  other arithmetic  9.15 us (4%)
    all_gather x1, waiting for transfers between devices, turned_gather(): out = lax.all_gather(both, axis, axis=0, tiled=True)  40.5 us
    all_gather x1, waiting for transfers between devices, body(): pieces = lax.all_gather(arrived, 'tp', axis=2, tiled=True)  36.1 us
    all_to_all x1, waiting for transfers between devices, copy_for_each(): return lax.all_to_all(copies, axis, split_axis=0, concat_axis=0, tiled=True)  31.1 us
    all_gather x1, blocking collectives, body(): lax.all_gather(head_out, 'tp', axis=1, tiled=True)  21 us
    all_gather x1, blocking collectives, body(): full_rows = lax.all_gather(hidden_state, 'tp', axis=1, tiled=True)  17.1 us
    all_to_all x1, blocking collectives, body(): lax.all_to_all(outgoing, 'sp', split_axis=0, concat_axis=1, tiled=True)  15.2 us
    all_to_all x1, starting transfers between devices, copy_for_each(): return lax.all_to_all(copies, axis, split_axis=0, concat_axis=0, tiled=True)  13.8 us
    all_to_all x1, starting transfers between devices, body(): lax.all_to_all(expert_add.astype(jnp.bfloat16), 'sp', split_axis=1, conca...  9.91 us
  transfers between devices with their start and end apart: 4, of which 4 were waited for; matrix products, arithmetic and copies ran while one was open for 3% of the time, Pallas kernels for 0%

commit v1 on v0

v1 whole, which is shorter than its diff:
```python
import jax
import jax.numpy as jnp
from jax import lax
from jax.experimental import pallas as pl
from jax.experimental.pallas import tpu as pltpu
from jax.sharding import PartitionSpec as P

MESH = pl.DeviceIdType.MESH
EPS = 1e-06
MASKED = -1e30
NX, NZ, NY, NT = 4, 8, 8, 16
NSP = NX * NZ
S = 192
HS = S // 2
SLOT = 16
ROWS = NSP * SLOT
D = 2048
CW = 128
LOG2E = 1.4426950408889634
BF = jnp.bfloat16
F32 = jnp.float32
CP = 2
EP = 4
FP = 2


def kernel(
    res_ref, q_ref, k_ref, v_ref, mw_ref, hg_ref, ng_ref, ids_ref, rw_ref,
    wo_hbm, eg_hbm, eu_hbm, ed_hbm, sg_hbm, su_hbm, sd_hbm,
    out_ref,
    kvall, qbig, m_s, l_s, acc, wo, wgu, wd, sgu, sd, m0, m1,
    hb, hfull, hid, hidall, normed, sb, outg, eb, fb, hidx, res_o, ret,
    wsem, asend, zup, zdn, xsem, bsend, bring, bpair, csend, cup, cdn, cpair,
    ssend, sring, spair, dsend, drecv, esend, eup, edn, epair,
    fsend, fup, fdn, fpair, gsend, grecv,
):
    sp = lax.axis_index("sp")
    tp = lax.axis_index("tp")
    z, x = sp // NX, sp % NX
    y, c = tp // 2, tp % 2
    pair_dev = (sp, y * 2 + (1 - c))

    def zdev(step):
        return ((z + step + NZ) % NZ * NX + x, tp)

    def xdev(step):
        return (z * NX + (x + step + NX) % NX, tp)

    def ydev(step):
        return (sp, (y + step + NY) % NY * 2 + c)

    def rcopy(src, dst, ssem, rsem, dev):
        return pltpu.make_async_remote_copy(
            src_ref=src, dst_ref=dst, send_sem=ssem, recv_sem=rsem,
            device_id=dev, device_id_type=MESH,
        )

    def wait_bytes(view, sem):
        pltpu.make_async_copy(view, view, sem).wait()

    loads = [
        pltpu.make_async_copy(wo_hbm, wo, wsem.at[0]),
        pltpu.make_async_copy(eg_hbm.at[0], wgu.at[0:64], wsem.at[1]),
        pltpu.make_async_copy(eu_hbm.at[0], wgu.at[64:128], wsem.at[2]),
        pltpu.make_async_copy(ed_hbm.at[0], wd, wsem.at[3]),
        pltpu.make_async_copy(sg_hbm, sgu.at[0:64], wsem.at[4]),
        pltpu.make_async_copy(su_hbm, sgu.at[64:128], wsem.at[5]),
        pltpu.make_async_copy(sd_hbm, sd, wsem.at[6]),
    ]
    for load in loads:
        load.start()

    barrier = pltpu.get_barrier_semaphore()

    def greet_sp(i, carry):
        pl.semaphore_signal(barrier, inc=1, device_id=((sp + i) % NSP, tp), device_id_type=MESH)
        return carry

    def greet_tp(i, carry):
        pl.semaphore_signal(barrier, inc=1, device_id=(sp, (tp + i) % NT), device_id_type=MESH)
        return carry

    lax.fori_loop(1, NSP, greet_sp, 0)
    lax.fori_loop(1, NT, greet_tp, 0)

    kvall[sp] = jnp.concatenate([k_ref[...], v_ref[...]], axis=1)
    q = q_ref[...]
    lane64 = lax.broadcasted_iota(jnp.int32, (S, 64), 1)
    zero64 = jnp.zeros((S, 64), BF)
    q1 = jnp.where(lane64 < 32, q, zero64)
    q2 = jnp.where(lane64 >= 32, q, zero64)
    qbig[0:S, :] = jnp.concatenate([q1, zero64], axis=1)
    qbig[S:, :] = jnp.concatenate([q2, zero64], axis=1)
    m_s[...] = jnp.full((2 * S, CW), MASKED, F32)
    l_s[...] = jnp.zeros((2 * S, CW), F32)
    acc[...] = jnp.zeros((2 * S, CW), F32)

    pl.semaphore_wait(barrier, NSP - 1 + NT - 1)

    def slot(step, xs=0):
        return (z + step + NZ) % NZ * NX + (x + xs + NX) % NX

    def z_up(k):
        r = kvall.at[slot(-k)]
        return rcopy(r, r, asend.at[0], zup.at[k], zdev(1))

    def z_dn(k):
        r = kvall.at[slot(k)]
        return rcopy(r, r, asend.at[0], zdn.at[k], zdev(-1))

    steps = [0]
    for k in range(4):
        steps.append(-1 - k)
        if k < 3:
            steps.append(1 + k)

    def x_right(n):
        r = kvall.at[slot(steps[n])]
        return rcopy(r, r, asend.at[0], xsem.at[n, 0], xdev(1))

    def x_left(n):
        r = kvall.at[slot(steps[n])]
        return rcopy(r, r, asend.at[0], xsem.at[n, 1], xdev(-1))

    def relay_right(n):
        r = kvall.at[slot(steps[n], -1), 0:HS]
        return rcopy(r, r, asend.at[0], xsem.at[n, 2], xdev(1))

    def relay_left(n):
        r = kvall.at[slot(steps[n], 1), HS:S]
        return rcopy(r, r, asend.at[0], xsem.at[n, 3], xdev(-1))

    def x_send(n):
        x_right(n).start()
        x_left(n).start()

    def x_relay(n):
        x_right(n).wait_recv()
        relay_right(n).start()
        x_left(n).wait_recv()
        relay_left(n).start()

    def x_finish(n):
        relay_right(n).wait_recv()
        relay_left(n).wait_recv()

    scale2 = LOG2E * 32.0 ** (-0.5)

    def attend(step, own):
        zj = (z + step + NZ) % NZ
        kv = kvall[pl.ds(zj * NX, NX)].reshape(NX * S, CW)
        s = lax.dot_general(qbig[...], kv, (((1,), (1,)), ((), ())), preferred_element_type=F32)
        if own:
            row = lax.broadcasted_iota(jnp.int32, (2 * S, NX * S), 0)
            row = jnp.where(row >= S, row - S, row) + x * S
            col = lax.broadcasted_iota(jnp.int32, (2 * S, NX * S), 1)
            s = jnp.where(col <= row, s, MASKED)
        m_old = m_s[:, 0:1]
        m_new = jnp.maximum(m_old, jnp.max(s, axis=1, keepdims=True))
        alpha = jnp.exp2((m_old - m_new) * scale2)
        p = jnp.exp2((s - m_new) * scale2)
        l_new = l_s[:, 0:1] * alpha + jnp.sum(p, axis=1, keepdims=True)
        pv = jnp.dot(p.astype(BF), kv, preferred_element_type=F32)
        acc[...] = acc[...] * alpha + pv
        m_s[...] = jnp.broadcast_to(m_new, (2 * S, CW))
        l_s[...] = jnp.broadcast_to(l_new, (2 * S, CW))

    def attend_group(n):
        if steps[n] == 0:
            attend(0, True)
        else:

            @pl.when((z + steps[n] + NZ) % NZ < z)
            def _():
                attend(steps[n], False)

    z_up(0).start()
    z_dn(0).start()
    x_send(0)

    lanes = lax.broadcasted_iota(jnp.int32, (S, CW), 1)
    id0, id1 = ids_ref[:, 0:1], ids_ref[:, 1:2]
    oh0 = jnp.where(lanes == id0, 1.0, 0.0).astype(F32)
    oh1 = jnp.where(lanes == id1, 1.0, 0.0).astype(F32)
    low = jnp.where(
        lax.broadcasted_iota(jnp.int32, (S, S), 1) < lax.broadcasted_iota(jnp.int32, (S, S), 0),
        1.0, 0.0,
    ).astype(BF)
    cum = jnp.dot(low, (oh0 + oh1).astype(BF), preferred_element_type=F32)
    slots = lax.broadcasted_iota(jnp.int32, (S, ROWS), 1).astype(F32)
    for ident, oh, m in ((id0, oh0, m0), (id1, oh1, m1)):
        at = ident.astype(F32) * SLOT + jnp.sum(oh * cum, axis=1, keepdims=True)
        m[...] = jnp.where(slots == at, 1.0, 0.0).astype(BF)

    groups = [[0]]
    for k in range(4):
        groups.append([2 * k + 1] + ([2 * k + 2] if k < 3 else []))
    for k in range(4):
        got = kvall.at[slot(-1 - k)]
        rcopy(got, got, asend.at[0], zup.at[k], zdev(1)).wait_recv()
        if k < 3:
            z_up(k + 1).start()
        x_send(2 * k + 1)
        if k < 3:
            got = kvall.at[slot(1 + k)]
            rcopy(got, got, asend.at[0], zdn.at[k], zdev(-1)).wait_recv()
            if k < 2:
                z_dn(k + 1).start()
            x_send(2 * k + 2)
        for n in groups[k]:
            x_relay(n)
        if k >= 1:
            for n in groups[k - 1]:
                x_finish(n)
                attend_group(n)
    for n in groups[4]:
        x_relay(n)
    for g in (3, 4):
        for n in groups[g]:
            x_finish(n)
            attend_group(n)

    summed = acc[...] / l_s[...]
    diff = summed[0:S] - mw_ref[0] * summed[S:]
    lane = lax.broadcasted_iota(jnp.int32, (S, CW), 1)
    squares = jnp.sum(jnp.where(lane >= 64, diff * diff, 0.0), axis=1, keepdims=True) * (1.0 / 64)
    gain = hg_ref[...]
    head_out = (diff * lax.rsqrt(squares + EPS))[:, 64:] * gain
    hb[tp] = jnp.concatenate([head_out[0:HS], head_out[HS:]], axis=1).astype(BF)

    def direct_gather(buf, send, ring, pair):
        mine = buf.at[tp]
        for i in range(1, NY):
            rcopy(mine, mine, send.at[0], ring.at[i], ydev(i)).start()
        rcopy(mine, mine, send.at[0], pair.at[0], pair_dev).start()

    def direct_finish(buf, send, ring, pair):
        for i in (1, 7, 2, 6, 3, 5, 4):
            got = buf.at[(y - i + NY) % NY * 2 + c]
            rcopy(got, got, send.at[0], ring.at[i], ydev(i)).wait_recv()
            rcopy(got, got, send.at[0], pair.at[0], pair_dev).start()
        wait_bytes(buf.at[0:NY], pair.at[0])

    direct_gather(hb, bsend, bring, bpair)
    direct_finish(hb, bsend, bring, bpair)

    loads[0].wait()
    for j in range(NY):
        a, b = hb[2 * j], hb[2 * j + 1]
        hfull[0:HS, 128 * j : 128 * j + 128] = jnp.concatenate([a[:, :64], b[:, :64]], axis=1)
        hfull[HS:, 128 * j : 128 * j + 128] = jnp.concatenate([a[:, 64:], b[:, 64:]], axis=1)
    attn = jnp.dot(hfull[...], wo[...], preferred_element_type=F32)
    hidden = (res_ref[...].astype(F32) + attn).astype(BF)
    hid[...] = hidden
    own_cols = pl.ds(pl.multiple_of(tp * CW, CW), CW)
    hidall[:, own_cols] = hidden

    def ring_gather(view, total, parts, send, up, dn, pair, ready=None):
        def one(t, p, sem, dev):
            r = view(t, p)
            return rcopy(r, r, send.at[0], sem, dev)

        for p in range(parts):
            if ready is not None:
                ready(p)
            one(tp, p, up.at[p], ydev(1)).start()
            one(tp, p, dn.at[p], ydev(-1)).start()
            one(tp, p, pair.at[0], pair_dev).start()
        for k in range(4):
            for p in range(parts):
                for going_up in (True, False):
                    first = p < parts // 2
                    if k == 3 and first != going_up:
                        continue
                    step, sem = (1, up) if going_up else (-1, dn)
                    t = (y - step * (1 + k) + NY) % NY * 2 + c
                    one(t, p, sem.at[k * parts + p], ydev(step)).wait_recv()
                    if k < 2 or (k == 2 and first == going_up):
                        one(t, p, sem.at[(k + 1) * parts + p], ydev(step)).start()
                    one(t, p, pair.at[0], pair_dev).start()
        wait_bytes(total, pair.at[0])

    def c_view(t, p):
        rows = S // CP
        return hidall.at[p * rows : (p + 1) * rows, pl.ds(pl.multiple_of(t * CW, CW), CW)]

    ring_gather(c_view, hidall.at[:, 0:1024], CP, csend, cup, cdn, cpair)

    for r in range(2):
        full = hidall[r * HS : (r + 1) * HS, :].astype(F32)
        sq = jnp.mean(full * full, axis=1, keepdims=True)
        normed[r * HS : (r + 1) * HS, :] = (full * lax.rsqrt(sq + EPS) * ng_ref[...]).astype(BF)

    both = m0[...] + m1[...]
    picked = lax.dot_general(
        both, normed[:, own_cols], (((0,), (0,)), ((), ())), preferred_element_type=F32
    ).astype(BF)
    outg[...] = picked.reshape(NSP, SLOT, CW)
    own_rows = pl.ds(pl.multiple_of(sp * SLOT, SLOT), SLOT)
    eb_own = eb.at[own_rows, own_cols]
    eb_own[...] = outg[sp]

    def send_block(i, carry):
        e = (sp + i) % NSP
        rcopy(outg.at[e], eb.at[own_rows, own_cols], dsend.at[0], drecv.at[z // 2], (e, tp)).start()
        return carry

    lax.fori_loop(1, NSP, send_block, 0)

    def gated(gu):
        g = gu[:, 0:64]
        u = gu[:, 64:128]
        return g / (1.0 + jnp.exp(-g)) * u

    loads[4].wait()
    loads[5].wait()
    gu = lax.dot_general(
        normed[...], sgu[...], (((1,), (1,)), ((), ())), preferred_element_type=F32
    )
    h = gated(gu)
    sb[tp] = jnp.concatenate([h[0:HS], h[HS:]], axis=1).astype(BF)
    direct_gather(sb, ssend, sring, spair)

    prow = ROWS // EP

    def e_view(t, p):
        return eb.at[p * prow : (p + 1) * prow, pl.ds(pl.multiple_of(t * CW, CW), CW)]

    def e_ready(p):
        n = prow // SLOT

        @pl.when(z // 2 == p)
        def _():
            wait_bytes(outg.at[0 : n - 1], drecv.at[p])

        @pl.when(z // 2 != p)
        def _():
            wait_bytes(outg.at[0:n], drecv.at[p])

    ring_gather(e_view, eb.at[:, 0:1024], EP, esend, eup, edn, epair, e_ready)

    loads[1].wait()
    loads[2].wait()
    for r in range(2):
        lo, hi = [
            gated(
                lax.dot_general(
                    eb[r * 128 + o : r * 128 + o + 128, :], wgu[...],
                    (((1,), (1,)), ((), ())), preferred_element_type=F32,
                )
            )
            for o in (0, 256)
        ]
        fb[tp, r * 128 : (r + 1) * 128, :] = jnp.concatenate([lo, hi], axis=1).astype(BF)

    def f_view(t, p):
        rows = 256 // FP
        return fb.at[t, p * rows : (p + 1) * rows]

    ring_gather(f_view, fb.at[0:NY], FP, fsend, fup, fdn, fpair)

    loads[3].wait()
    for j in range(NY):
        a, b = fb[2 * j], fb[2 * j + 1]
        hidx[0:256, 128 * j : 128 * j + 128] = jnp.concatenate([a[:, :64], b[:, :64]], axis=1)
        hidx[256:, 128 * j : 128 * j + 128] = jnp.concatenate([a[:, 64:], b[:, 64:]], axis=1)
    for r in range(2):
        res = jnp.dot(hidx[r * 256 : (r + 1) * 256, :], wd[...], preferred_element_type=F32)
        res_o[r * 16 : (r + 1) * 16] = res.astype(BF).reshape(16, SLOT, CW)

    ret[sp] = res_o[sp]

    def return_block(i, carry):
        e = (sp + i) % NSP
        rcopy(res_o.at[e], ret.at[sp], gsend.at[0], grecv.at[0], (e, tp)).start()
        return carry

    lax.fori_loop(1, NSP, return_block, 0)

    direct_finish(sb, ssend, sring, spair)
    loads[6].wait()
    for j in range(NY):
        a, b = sb[2 * j], sb[2 * j + 1]
        hfull[0:HS, 128 * j : 128 * j + 128] = jnp.concatenate([a[:, :64], b[:, :64]], axis=1)
        hfull[HS:, 128 * j : 128 * j + 128] = jnp.concatenate([a[:, 64:], b[:, 64:]], axis=1)
    shared = jnp.dot(hfull[...], sd[...], preferred_element_type=F32)
    base = hid[...].astype(F32) + shared

    wait_bytes(outg.at[0 : NSP - 1], grecv.at[0])
    back = ret[...].reshape(ROWS, CW)
    r0 = jnp.dot(m0[...], back, preferred_element_type=F32)
    r1 = jnp.dot(m1[...], back, preferred_element_type=F32)
    routed = r0 * rw_ref[:, 0:1] + r1 * rw_ref[:, 1:2]
    out_ref[...] = (base + routed).astype(BF)

    wait_bytes(kvall.at[0 : NSP - 1], asend.at[0])
    wait_bytes(hb.at[0 : NT - 1], bsend.at[0])
    wait_bytes(hidall.at[:, 0 : 15 * CW], csend.at[0])
    wait_bytes(sb.at[0 : NT - 1], ssend.at[0])
    wait_bytes(outg.at[0 : NSP - 1], dsend.at[0])
    wait_bytes(eb.at[:, 0 : 15 * CW], esend.at[0])
    wait_bytes(fb.at[0 : NT - 1], fsend.at[0])
    wait_bytes(outg.at[0 : NSP - 1], gsend.at[0])


def body(
    residual_in, query_rows, key_rows, value_rows, map_weight, head_gain, out_proj, norm_gain,
    route_ids, route_weights, expert_gate, expert_up, expert_down, shared_gate, shared_up,
    shared_down,
):
    vm = pl.BlockSpec(memory_space=pltpu.VMEM)
    sm = pl.BlockSpec(memory_space=pltpu.SMEM)
    anyw = pl.BlockSpec(memory_space=pl.ANY)
    dma = pltpu.SemaphoreType.DMA
    v = pltpu.VMEM
    return pl.pallas_call(
        kernel,
        name="layer",
        out_shape=jax.ShapeDtypeStruct((S, CW), BF),
        in_specs=[vm, vm, vm, vm, sm, vm, vm, vm, vm] + [anyw] * 7,
        out_specs=vm,
        scratch_shapes=[
            v((NSP, S, CW), BF),
            v((2 * S, CW), BF),
            v((2 * S, CW), F32),
            v((2 * S, CW), F32),
            v((2 * S, CW), F32),
            v((1024, CW), BF),
            v((128, D), BF),
            v((1024, CW), BF),
            v((128, D), BF),
            v((1024, CW), BF),
            v((S, ROWS), BF),
            v((S, ROWS), BF),
            v((NT, HS, CW), BF),
            v((S, 1024), BF),
            v((S, CW), BF),
            v((S, D), BF),
            v((S, D), BF),
            v((NT, HS, CW), BF),
            v((NSP, SLOT, CW), BF),
            v((ROWS, D), BF),
            v((NT, 256, CW), BF),
            v((ROWS, 1024), BF),
            v((NSP, SLOT, CW), BF),
            v((NSP, SLOT, CW), BF),
            dma((7,)),
            dma((1,)), dma((4,)), dma((3,)), dma((8, 4)),
            dma((1,)), dma((8,)), dma((1,)),
            dma((1,)), dma((4 * CP,)), dma((4 * CP,)), dma((1,)),
            dma((1,)), dma((8,)), dma((1,)),
            dma((1,)), dma((EP,)),
            dma((1,)), dma((4 * EP,)), dma((4 * EP,)), dma((1,)),
            dma((1,)), dma((4 * FP,)), dma((4 * FP,)), dma((1,)),
            dma((1,)), dma((1,)),
        ],
        compiler_params=pltpu.CompilerParams(
            collective_id=0, has_side_effects=True, vmem_limit_bytes=60 * 1024 * 1024
        ),
    )(
        residual_in, query_rows, key_rows, value_rows, map_weight,
        head_gain.reshape(1, 64), norm_gain.reshape(1, D), route_ids, route_weights,
        out_proj, expert_gate, expert_up, expert_down, shared_gate, shared_up, shared_down,
    )


def solution(mesh):
    in_specs = (
        P("sp", "tp"),
        P("sp", "tp"),
        P("sp", "tp"),
        P("sp", "tp"),
        P("tp"),
        P(),
        P(None, "tp"),
        P(),
        P("sp", None),
        P("sp", None),
        P("sp", "tp", None),
        P("sp", "tp", None),
        P("sp", None, "tp"),
        P("tp", None),
        P("tp", None),
        P(None, "tp"),
    )
    return jax.shard_map(
        body, mesh=mesh, in_specs=in_specs, out_specs=P("sp", "tp"), check_vma=False
    )
```

time: 246 us -> 114 us (0.46)
  waiting for transfers between devices: 117 us -> 0 us
  Pallas kernels: 0 us -> 107 us
  blocking collectives: 53.3 us -> 0 us
  starting transfers between devices: 23.8 us -> 0 us
  matrix products: 14.5 us -> 0 us
  between operations: 14.5 us -> 0.68 us
  other arithmetic: 9.15 us -> 0 us
  local copies, waits for them, and re-layouts: 13.1 us -> 5.92 us
    pallas_call x0 -> x1, Pallas kernels: none -> 107 us  [body(): pl.pallas_call(kernel, name='layer', out_shape=jax.ShapeDtypeStruct((S, C...]
    all_gather x2 -> x0, waiting for transfers between devices: 76.7 us -> none  [the longest x1 40.5 us: turned_gather(): out = lax.all_gather(both, axis, axis=0, tiled=True)]
    all_to_all x2 -> x0, waiting for transfers between devices: 40.3 us -> none  [the longest x1 31.1 us: copy_for_each(): return lax.all_to_all(copies, axis, split_axis=0, concat_axis=0, tiled=True)]
    all_gather x2 -> x0, blocking collectives: 38.1 us -> none  [the longest x1 21 us: body(): lax.all_gather(head_out, 'tp', axis=1, tiled=True)]
    all_to_all x2 -> x0, starting transfers between devices: 23.7 us -> none  [the longest x1 13.8 us: copy_for_each(): return lax.all_to_all(copies, axis, split_axis=0, concat_axis=0, tiled=True)]
    all_to_all x1 -> x0, blocking collectives: 15.2 us -> none  [body(): lax.all_to_all(outgoing, 'sp', split_axis=0, concat_axis=1, tiled=True)]
    dot_general x9 -> x0, matrix products: 14.5 us -> none  [the longest x1 3.55 us: body(): jnp.einsum('qhmd,khmd->mhqk', query_heads, key_heads, preferred_element_t...]
    unnamed x34 -> x14, local copies, waits for them, and re-layouts: 1.79 us -> 5.92 us
  transfers between devices with their start and end apart: 4 -> 0, of which waited for: 4 -> 0; matrix products, arithmetic and copies ran while one was open for 3% -> 0% of each run, Pallas kernels for 0% -> 0%
where the time goes in v1:
time: 114 us; the launch traced here: 113 us
  Pallas kernels  107 us (94%)
  local copies, waits for them, and re-layouts  5.92 us (5%)
    pallas_call x1, Pallas kernels, body(): pl.pallas_call(kernel, name='layer', out_shape=jax.ShapeDtypeStruct((S, C...  107 us
    unnamed x14, local copies, waits for them, and re-layouts  5.92 us

profile of v1, /device:TPU:1, one launch (start us, length us, event | category | flops | bytes accessed | tf_op | source)
XLA Modules:
  0.0 113.4 jit_solution(3147583390048251001)
XLA Ops:
  0.7 0.0 copy-start
  0.7 1.5 %copy.17.q_ref = bf16[192,64]{1,0:T(8,128)(2,1)} copy(bf16[192,64]{0,1:T(8,128)(2,1)} %param.17) | data formatting | bytes 49152 | tf_op args[1]
  2.1 0.0 copy-done
  2.1 0.0 copy-start.1
  2.2 0.7 copy.18.k_ref
  2.9 0.0 copy-done.1
  2.9 0.0 copy-start.2
  2.9 0.7 copy.19.v_ref
  3.6 0.0 copy-done.2
  3.6 0.0 copy-start.3
  3.6 0.8 copy.20.ids_ref
  4.4 0.0 copy-done.3
  4.4 0.8 copy.21.rw_ref
  5.2 106.8 %layer.1 = bf16[192,128]{1,0:T(8,128)(2,1)} custom-call(bf16[192,128]{1,0:T(8,128)(2,1)} %res_ref.1, bf16[192,64]{1,0:T(8,128)(2,1)} %copy.17.q_ref, bf16[192,64]{1,0:T(8,128)(2,1)} %copy.18.k_ref, bf16[192,64]{1,0:T(8,128)(2,1)} %copy.19.v_ref, f32[1]{0:T(128)S(6)} %copy.23.mw_ref, f32[1,64]{1,0:T(1,128)} %bitcast.3, f32[1,2048]{1,0:T(1,128)} %bitcast.2, ...), custom_call_target="tpu_custom_call" | custom-call | tf_op jit(solution)/shard_map/layer/pallas_call | solution.py:416
  111.9 1.4 %copy.24 = bf16[192,128]{1,0:T(8,128)(2,1)} copy(bf16[192,128]{1,0:T(8,128)(2,1)} %layer.1) | data formatting | bytes 98304
Async XLA Ops:
  0.7 1.5 %copy-start = (bf16[192,64]{0,1:T(8,128)(2,1)S(1)}, bf16[192,64]{0,1:T(8,128)(2,1)}, u32[]{:S(2)}) copy-start(bf16[192,64]{0,1:T(8,128)(2,1)} %param.18) | copy-start | bytes 73732
  2.1 0.8 copy-start.1
  2.9 0.7 copy-start.2
  3.6 0.8 copy-start.3
